TPU v7x, 32 devices: a whole 2x2x4 slice. The times are simulated.
32 devices in a mesh: fs: 4 (over y, x), tp: 8 (over z, core).
Axes of the slice: x: 2, y: 2, z: 4, core: 2. Of those that a mesh axis runs over, the one named last changes fastest.
Arguments:
- tokens: bfloat16 [1024, 2048], P('fs', 'tp'), may hold values from -60 to 60
- norm_gain: float32 [2048], P('fs'), may hold values from 0.1 to 1.9
- gate_weight: float32 [4, 2048, 4096], P(None, 'fs', 'tp'), may hold values from -0.125 to 0.125
- up_weight: float32 [4, 2048, 4096], P(None, 'fs', 'tp'), may hold values from -0.125 to 0.125
- down_weight: float32 [4, 2048, 4096], P(None, 'fs', 'tp'), may hold values from -0.125 to 0.125
- route: int32 [1024, 2], P('fs'), may hold values from 0 to 3, all different within a row; in each aligned block of 256 rows (0 to 255, 256 to 511, ...) at most 256 rows name the same one
- route_weight: float32 [1024, 2], P('fs'), may hold values from 0.2 to 1
Outputs:
- mixed: bfloat16 [1024, 2048], P('fs', 'tp')
- gate_new: bfloat16 [4, 2048, 4096], P('fs', None, 'tp')
- up_new: bfloat16 [4, 2048, 4096], P('fs', None, 'tp')
- down_new: bfloat16 [4, 2048, 4096], P('fs', None, 'tp')
Inputs may be any that keep to these rules, and one draw needn't show every extreme that they name: `route`: the 2 experts of a row differ. In each aligned block of 256 rows (the tokens of one index of fs) no expert is named by more than 256 rows, a bound that some block reaches.
All inputs are finite; a program needn't handle non-finite values.
Results may differ from a plain program's by a relative error of at most 0.024.
Values may be sent and summed in bfloat16 or wider, within the bound.
A program may use at most 64 MiB of HBM per device.

v0:
```python
import jax
import jax.numpy as jnp
from jax import lax
from jax.sharding import PartitionSpec as P

epsilon = 1e-05


def slot_table(route, block_rows, expert_count):
    pair_ids = route.reshape(-1, block_rows * route.shape[1])
    onehot = (
        pair_ids[:, :, None] == jnp.arange(expert_count, dtype=jnp.int32)[None, None, :]
    ).astype(jnp.int32)
    before = jnp.cumsum(onehot, axis=1) - onehot
    return jnp.sum(before * onehot, axis=2).reshape(route.shape)


def body(tokens, norm_gain, gate_weight, up_weight, down_weight, route, route_weight):
    experts = gate_weight.shape[0]
    tok_rows = tokens.shape[0]
    columns = tokens.shape[1]
    fs_count = lax.axis_size("fs")
    capacity = 4 * tok_rows // fs_count
    gain_col = norm_gain[None, :, None]
    gate_cast = (gate_weight * gain_col).astype(jnp.bfloat16)
    up_cast = (up_weight * gain_col).astype(jnp.bfloat16)
    down_cast = down_weight.astype(jnp.bfloat16)
    gate_new, up_new, down_new = (
        lax.all_to_all(gate_cast, "fs", split_axis=0, concat_axis=1, tiled=True),
        lax.all_to_all(up_cast, "fs", split_axis=0, concat_axis=1, tiled=True),
        lax.all_to_all(down_cast, "fs", split_axis=0, concat_axis=1, tiled=True),
    )
    slot_of = slot_table(route, tok_rows, experts)
    target = route * capacity + slot_of
    slot_lanes = jnp.arange(experts * capacity, dtype=jnp.int32)
    slot_hits = target[:, :, None] == slot_lanes[None, None, :]
    token_iota = jnp.arange(tok_rows, dtype=jnp.int32)[:, None, None]
    lane_token = jnp.sum(jnp.where(slot_hits, token_iota + 1, 0), axis=(0, 1)) - 1
    lane_token = jnp.where(lane_token < 0, tok_rows, lane_token)
    combine = jnp.sum(jnp.where(slot_hits, route_weight[:, :, None], 0.0), axis=1)
    tok_float = tokens.astype(jnp.float32)
    square_sum = lax.psum(jnp.sum(tok_float * tok_float, axis=1), "tp")
    full_width = columns * lax.axis_size("tp")
    normed = (tok_float * lax.rsqrt(square_sum / full_width + epsilon)[:, None]).astype(
        jnp.bfloat16
    )
    padded = jnp.concatenate([normed, jnp.zeros((1, columns), jnp.bfloat16)], axis=0)
    outgoing = padded[lane_token].reshape(experts, capacity, columns)
    arrived = lax.all_to_all(outgoing, "fs", split_axis=0, concat_axis=0, tiled=True).reshape(
        -1, columns
    )
    gate_local = gate_new[0]
    up_local = up_new[0]
    piece_rows = lax.all_gather(arrived, "tp", axis=1, tiled=True)
    gate_acc = jnp.dot(piece_rows, gate_local, preferred_element_type=jnp.float32)
    up_acc = jnp.dot(piece_rows, up_local, preferred_element_type=jnp.float32)
    hidden = (jax.nn.silu(gate_acc) * up_acc).astype(jnp.bfloat16)
    down_local = down_new[0]
    summed = lax.psum_scatter(
        lax.dot_general(
            down_local, hidden, (((1,), (1,)), ((), ())), preferred_element_type=jnp.float32
        ).astype(jnp.bfloat16),
        "tp",
        scatter_dimension=0,
        tiled=True,
    ).astype(jnp.float32)
    own_columns = summed.shape[0]
    outgoing_back = summed.astype(jnp.bfloat16).reshape(own_columns, fs_count, capacity)
    returned = lax.all_to_all(outgoing_back, "fs", split_axis=1, concat_axis=1, tiled=True).reshape(
        own_columns, experts * capacity
    )
    mixed = lax.dot_general(
        combine,
        returned.astype(jnp.float32),
        (((1,), (1,)), ((), ())),
        precision=lax.Precision.HIGHEST,
        preferred_element_type=jnp.float32,
    )
    return (mixed.astype(jnp.bfloat16), gate_new, up_new, down_new)


def solution(mesh):
    in_specs = (
        P("fs", "tp"),
        P("fs"),
        P(None, "fs", "tp"),
        P(None, "fs", "tp"),
        P(None, "fs", "tp"),
        P("fs", None),
        P("fs", None),
    )
    out_specs = (P("fs", "tp"), P("fs", None, "tp"), P("fs", None, "tp"), P("fs", None, "tp"))
    return jax.shard_map(body, mesh=mesh, in_specs=in_specs, out_specs=out_specs, check_vma=False)
```

profile of v0, /device:TPU:0, one launch (start us, length us, event | category | flops | bytes accessed | tf_op | source)
XLA Modules:
  0.0 224.2 jit_solution(16390866846317587679)
XLA Ops:
  7.2 0.8 copy.21
  8.2 1.2 reduce-window.6
  10.2 0.7 multiply_add_fusion
  11.2 1.0 fusion
  12.2 18.1 %psum.7 = f32[256]{0:T(256)S(1)} all-reduce(f32[256]{0:T(256)S(1)} %fusion), channel_id=1, replica_groups=mesh['fs'=4,'tp'=8] {'tp'}, use_global_device_ids=true, to_apply=%region_5.6 | all-reduce | flops 256 | bytes 2048 | tf_op jit(solution)/shard_map/psum | solution.py:42
  30.4 1.0 fusion.1
  31.4 3.9 %gather_fusion = bf16[1024,256]{1,0:T(8,128)(2,1)S(1)} fusion(bf16[257,256]{1,0:T(8,128)(2,1)S(1)} %concatenate.3, s32[1024]{0:T(1024)S(1)} %broadcast_clamp_fusion), kind=kCustom, calls=%fused_computation | custom fusion | bytes 1052672 | tf_op jit(solution)/shard_map/gather | solution.py:48
  35.3 10.7 %all_to_all.46 = bf16[4,256,256]{2,1,0:T(8,128)(2,1)} all-to-all(bf16[4,256,256]{2,1,0:T(8,128)(2,1)S(1)} %bitcast.31), channel_id=1, replica_groups=mesh['fs'=4,'tp'=8] {'fs'}, dimensions={0} | all-to-all | bytes 1048576 | tf_op jit(solution)/shard_map/all_to_all | solution.py:49
  46.1 6.1 %multiply_convert_fusion = (bf16[4,512,512]{2,1,0:T(8,128)(2,1)}, bf16[4,512,512]{2,1,0:T(8,128)(2,1)S(1)}) fusion(f32[4,512,512]{2,1,0:T(8,128)} %param.10, f32[512]{0:T(512)S(1)} %copy-done.1, f32[4,512,512]{2,1,0:T(8,128)} %param.9), kind=kLoop, calls=%fused_computation.2 | loop fusion | flops 4194304 | bytes 12584960 | tf_op jit(solution)/shard_map/convert_element_type | solution.py:26
  52.3 23.8 %all_to_all.47 = bf16[4,512,512]{2,1,0:T(8,128)(2,1)S(1)} all-to-all(bf16[4,512,512]{2,1,0:T(8,128)(2,1)S(1)} %get-tuple-element.5), channel_id=1, replica_groups=mesh['fs'=4,'tp'=8] {'fs'}, dimensions={0} | all-to-all | bytes 4194304 | tf_op jit(solution)/shard_map/all_to_all | solution.py:29
  76.1 4.5 %all-to-all-start.2 = ((bf16[4,512,512]{2,1,0:T(8,128)(2,1)}), bf16[4,512,512]{2,1,0:T(8,128)(2,1)}, u32[]{:S(2)}, u32[]{:S(2)}) async-start(bf16[4,512,512]{2,1,0:T(8,128)(2,1)} %get-tuple-element.4), calls=%async_computation.2 | async-start | bytes 4194304 | tf_op jit(solution)/shard_map/all_to_all | solution.py:30
  80.6 3.8 %convert_element_type.47 = bf16[4,512,512]{2,1,0:T(8,128)(2,1)} convert(f32[4,512,512]{2,1,0:T(8,128)} %param.11) | non-fusion elementwise | flops 1048576 | bytes 6291456 | tf_op jit(solution)/shard_map/convert_element_type | solution.py:27
  84.4 16.0 %all-to-all-done.2 = bf16[4,512,512]{2,1,0:T(8,128)(2,1)} async-done(((bf16[4,512,512]{2,1,0:T(8,128)(2,1)}), bf16[4,512,512]{2,1,0:T(8,128)(2,1)}, u32[]{:S(2)}, u32[]{:S(2)}) %all-to-all-start.2) | async-done | bytes 2097184 | tf_op jit(solution)/shard_map/all_to_all | solution.py:30
  100.4 4.5 %all-to-all-start.3 = ((bf16[4,512,512]{2,1,0:T(8,128)(2,1)}), bf16[4,512,512]{2,1,0:T(8,128)(2,1)}, u32[]{:S(2)}, u32[]{:S(2)}) async-start(bf16[4,512,512]{2,1,0:T(8,128)(2,1)} %convert_element_type.47), calls=%async_computation.3 | async-start | bytes 4194304 | tf_op jit(solution)/shard_map/all_to_all | solution.py:31
  104.9 5.8 %fusion.5 = f32[1024,512]{1,0:T(8,128)} fusion(bf16[1024,2048]{1,0:T(8,128)(2,1)} %all-gather.2.cloned.1.call-done, bf16[2048,512]{1,0:T(8,128)(2,1)S(1)} %bitcast.28), kind=kOutput, calls=%fused_computation.28 | convolution fusion | flops 2147483648 | bytes 8388608 | tf_op jit(solution)/shard_map/dot_general | solution.py:55
  110.8 18.5 %all-to-all-done.3 = bf16[4,512,512]{2,1,0:T(8,128)(2,1)} async-done(((bf16[4,512,512]{2,1,0:T(8,128)(2,1)}), bf16[4,512,512]{2,1,0:T(8,128)(2,1)}, u32[]{:S(2)}, u32[]{:S(2)}) %all-to-all-start.3) | async-done | bytes 2097184 | tf_op jit(solution)/shard_map/all_to_all | solution.py:31
  129.3 10.6 %convert_bitcast_fusion = bf16[2048,1024]{0,1:T(8,128)(2,1)} fusion(bf16[2048,512]{1,0:T(8,128)(2,1)} %bitcast.9, f32[1024,512]{1,0:T(8,128)} %fusion.5, bf16[1024,2048]{1,0:T(8,128)(2,1)} %all-gather.2.cloned.1.call-done, bf16[2048,512]{1,0:T(8,128)(2,1)} %bitcast.8), kind=kOutput, calls=%fused_computation.1 | convolution fusion | flops 4300210176 | bytes 14680064 | tf_op jit(solution)/shard_map/dot_general | solution.py:60
  139.9 56.9 %reduce-scatter.2.cloned.1.call-done = bf16[256,1024]{0,1:T(8,128)(2,1)} async-done(((bf16[2048,1024]{0,1:T(8,128)(2,1)}), bf16[256,1024]{0,1:T(8,128)(2,1)}) %reduce-scatter.2.cloned.1.call-update) | async-done | bytes 524304 | tf_op jit(solution)/shard_map/reduce_scatter | solution.py:59
  196.8 4.1 %all-to-all-start.4 = ((bf16[256,4,256]{0,2,1:T(8,128)(2,1)}), bf16[256,4,256]{0,2,1:T(8,128)(2,1)}, u32[]{:S(2)}, u32[]{:S(2)}) async-start(bf16[256,4,256]{0,2,1:T(8,128)(2,1)} %bitcast.32), calls=%async_computation.5 | async-start | bytes 1048576 | tf_op jit(solution)/shard_map/all_to_all | solution.py:69
  201.3 6.4 %all-to-all-done.4 = bf16[256,4,256]{0,2,1:T(8,128)(2,1)} async-done(((bf16[256,4,256]{0,2,1:T(8,128)(2,1)}), bf16[256,4,256]{0,2,1:T(8,128)(2,1)}, u32[]{:S(2)}, u32[]{:S(2)}) %all-to-all-start.4) | async-done | bytes 524320 | tf_op jit(solution)/shard_map/all_to_all | solution.py:69
  207.6 2.3 %convolution_convert_fusion = bf16[256,256]{1,0:T(8,128)(2,1)} fusion(f32[256,1024]{1,0:T(8,128)S(1)} %select_reduce_fusion.1, bf16[256,1024]{0,1:T(8,128)(2,1)} %bitcast.12), kind=kOutput, calls=%fused_computation.8 | convolution fusion | flops 805371904 | bytes 1703936 | tf_op jit(solution)/shard_map/dot_general | solution.py:72
  209.9 1.3 copy.26
  211.3 3.0 %copy.27 = bf16[1,2048,512]{2,1,0:T(8,128)(2,1)} copy(bf16[1,2048,512]{2,1,0:T(8,128)(2,1)} %bitcast.14) | data formatting | bytes 4194304
  214.3 3.0 %copy.28 = bf16[1,2048,512]{2,1,0:T(8,128)(2,1)} copy(bf16[1,2048,512]{2,1,0:T(8,128)(2,1)} %bitcast.15) | data formatting | bytes 4194304
  (29 shorter events, 1.6 us)
Async XLA Ops:
  7.2 97.8 %all-gather.2.cloned.1.call-start = ((), (), s32[]{:S(2)}) async-start(), calls=%async_computation.6 | async-start | bytes 4718592 | tf_op jit(solution)/shard_map/all_gather | solution.py:54
  31.4 14.7 %copy-start.1 = (f32[512]{0:T(512)S(1)}, f32[512]{0:T(512)}, u32[]{:S(2)}) copy-start(f32[512]{0:T(512)} %param.8) | copy-start | bytes 6148
  76.1 24.3 %all-to-all-start.2 = ((bf16[4,512,512]{2,1,0:T(8,128)(2,1)}), bf16[4,512,512]{2,1,0:T(8,128)(2,1)}, u32[]{:S(2)}, u32[]{:S(2)}) async-start(bf16[4,512,512]{2,1,0:T(8,128)(2,1)} %get-tuple-element.4), calls=%async_computation.2 | async-start | bytes 4194304 | tf_op jit(solution)/shard_map/all_to_all | solution.py:30
  100.4 28.9 %all-to-all-start.3 = ((bf16[4,512,512]{2,1,0:T(8,128)(2,1)}), bf16[4,512,512]{2,1,0:T(8,128)(2,1)}, u32[]{:S(2)}, u32[]{:S(2)}) async-start(bf16[4,512,512]{2,1,0:T(8,128)(2,1)} %convert_element_type.47), calls=%async_computation.3 | async-start | bytes 4194304 | tf_op jit(solution)/shard_map/all_to_all | solution.py:31
  104.9 92.0 %reduce-scatter.2.cloned.1.call-start = ((), (), s32[]{:S(2)}) async-start(), calls=%async_computation.7 | async-start | bytes 4718592 | tf_op jit(solution)/shard_map/reduce_scatter | solution.py:59
  139.9 61.1 %copy-start = (f32[256,2]{0,1:T(2,128)S(1)}, f32[256,2]{0,1:T(2,128)}, u32[]{:S(2)}) copy-start(f32[256,2]{0,1:T(2,128)} %param.13) | copy-start | bytes 6148
  196.8 10.8 %all-to-all-start.4 = ((bf16[256,4,256]{0,2,1:T(8,128)(2,1)}), bf16[256,4,256]{0,2,1:T(8,128)(2,1)}, u32[]{:S(2)}, u32[]{:S(2)}) async-start(bf16[256,4,256]{0,2,1:T(8,128)(2,1)} %bitcast.32), calls=%async_computation.5 | async-start | bytes 1048576 | tf_op jit(solution)/shard_map/all_to_all | solution.py:69
Sparse Core Ops, SparseCore 0:
  46.2 44.4 all-gather.1
  140.0 56.7 reduce-scatter.1
where the time goes:
time: 225 us; the launch traced here: 224 us
  waiting for transfers between devices  97.9 us (44%)
  blocking collectives  52.7 us (23%)
  matrix products  18.7 us (8%)
  other arithmetic  14.6 us (6%)
  between operations  14.2 us (6%)
  starting transfers between devices  13.2 us (6%)
  local copies, waits for them, and re-layouts  12.9 us (6%)
    reduce_scatter x1, waiting for transfers between devices, body(): lax.psum_scatter(lax.dot_general(down_local, hidden, (((1,), (1,)), ((),...  56.9 us
    all_to_all x1, blocking collectives, body(): lax.all_to_all(gate_cast, 'fs', split_axis=0, concat_axis=1, tiled=True)  23.8 us
    all_to_all x1, waiting for transfers between devices, body(): lax.all_to_all(down_cast, 'fs', split_axis=0, concat_axis=1, tiled=True)  18.5 us
    psum x1, blocking collectives, body(): square_sum = lax.psum(jnp.sum(tok_float * tok_float, axis=1), 'tp')  18.1 us
    all_to_all x1, waiting for transfers between devices, body(): lax.all_to_all(up_cast, 'fs', split_axis=0, concat_axis=1, tiled=True)  16 us
    all_to_all x1, blocking collectives, body(): lax.all_to_all(outgoing, 'fs', split_axis=0, concat_axis=0, tiled=True)  10.7 us
    dot_general x1, matrix products, body(): lax.dot_general(down_local, hidden, (((1,), (1,)), ((), ())), preferred_e...  10.6 us
    unnamed x8, local copies, waits for them, and re-layouts  8.23 us
  transfers between devices with their start and end apart: 5, of which 4 were waited for; matrix products, arithmetic and copies ran while one was open for 7% of the time, Pallas kernels for 0%

commit v1 on v0

--- a/solution.py
+++ b/solution.py
@@ -28,7 +28,12 @@
     gate_new, up_new, down_new = (
         lax.all_to_all(gate_cast, "fs", split_axis=0, concat_axis=1, tiled=True),
         lax.all_to_all(up_cast, "fs", split_axis=0, concat_axis=1, tiled=True),
-        lax.all_to_all(down_cast, "fs", split_axis=0, concat_axis=1, tiled=True),
+        jnp.concatenate(
+            lax.all_to_all(
+                jnp.stack(jnp.split(down_cast, lax.axis_size("fs"), axis=0)), "fs", 0, 0
+            ),
+            axis=1,
+        ),
     )
     slot_of = slot_table(route, tok_rows, experts)
     target = route * capacity + slot_of

time: 225 us -> 228 us (1.013)
  waiting for transfers between devices: 97.9 us -> 90.7 us
  blocking collectives: 52.7 us -> 58.3 us
  local copies, waits for them, and re-layouts: 12.9 us -> 16.9 us
    all_to_all x1, blocking collectives: 23.8 us -> 29.5 us  [body(): lax.all_to_all(gate_cast, 'fs', split_axis=0, concat_axis=1, tiled=True)]
    all_to_all x1, waiting for transfers between devices: 18.5 us -> 14.1 us  [body(): lax.all_to_all(jnp.stack(jnp.split(down_cast, lax.axis_size('fs'), axis=0...]
    reduce_scatter x1, waiting for transfers between devices: 56.9 us -> 53.7 us  [body(): lax.psum_scatter(lax.dot_general(down_local, hidden, (((1,), (1,)), ((),...]
  transfers between devices with their start and end apart: 5 -> 5, of which waited for: 4 -> 4; matrix products, arithmetic and copies ran while one was open for 7% -> 8% of each run, Pallas kernels for 0% -> 0%
where the time goes in v1:
time: 228 us; the launch traced here: 227 us
  waiting for transfers between devices  90.7 us (40%)
  blocking collectives  58.3 us (26%)
  matrix products  18.9 us (8%)
  local copies, waits for them, and re-layouts  16.9 us (7%)
  other arithmetic  15.5 us (7%)
  between operations  14.2 us (6%)
  starting transfers between devices  12.5 us (5%)
    reduce_scatter x1, waiting for transfers between devices, body(): lax.psum_scatter(lax.dot_general(down_local, hidden, (((1,), (1,)), ((),...  53.7 us
    all_to_all x1, blocking collectives, body(): lax.all_to_all(gate_cast, 'fs', split_axis=0, concat_axis=1, tiled=True)  29.5 us
    psum x1, blocking collectives, body(): square_sum = lax.psum(jnp.sum(tok_float * tok_float, axis=1), 'tp')  18.1 us
    all_to_all x1, waiting for transfers between devices, body(): lax.all_to_all(up_cast, 'fs', split_axis=0, concat_axis=1, tiled=True)  16.6 us
    all_to_all x1, waiting for transfers between devices, body(): lax.all_to_all(jnp.stack(jnp.split(down_cast, lax.axis_size('fs'), axis=0...  14.1 us
    all_to_all x1, blocking collectives, body(): lax.all_to_all(outgoing, 'fs', split_axis=0, concat_axis=0, tiled=True)  10.7 us
    dot_general x1, matrix products, body(): lax.dot_general(down_local, hidden, (((1,), (1,)), ((), ())), preferred_e...  10.1 us
    unnamed x8, local copies, waits for them, and re-layouts  8.23 us
  transfers between devices with their start and end apart: 5, of which 4 were waited for; matrix products, arithmetic and copies ran while one was open for 8% of the time, Pallas kernels for 0%

profile of v1, /device:TPU:0, one launch (start us, length us, event | category | flops | bytes accessed | tf_op | source)
XLA Modules:
  0.0 227.1 jit_solution(15596830270283513134)
XLA Ops:
  8.2 1.2 reduce-window.6
  11.2 1.0 fusion
  12.2 18.1 %psum.7 = f32[256]{0:T(256)S(1)} all-reduce(f32[256]{0:T(256)S(1)} %fusion), channel_id=1, replica_groups=mesh['fs'=4,'tp'=8] {'tp'}, use_global_device_ids=true, to_apply=%region_5.6 | all-reduce | flops 256 | bytes 2048 | tf_op jit(solution)/shard_map/psum | solution.py:47
  31.4 3.9 %gather_fusion = bf16[1024,256]{1,0:T(8,128)(2,1)S(1)} fusion(bf16[257,256]{1,0:T(8,128)(2,1)S(1)} %concatenate.3, s32[1024]{0:T(1024)S(1)} %broadcast_clamp_fusion), kind=kCustom, calls=%fused_computation | custom fusion | bytes 1052672 | tf_op jit(solution)/shard_map/gather | solution.py:53
  35.3 10.7 %all_to_all.39 = bf16[4,256,256]{2,1,0:T(8,128)(2,1)} all-to-all(bf16[4,256,256]{2,1,0:T(8,128)(2,1)S(1)} %bitcast.43), channel_id=1, replica_groups=mesh['fs'=4,'tp'=8] {'fs'}, dimensions={0} | all-to-all | bytes 1048576 | tf_op jit(solution)/shard_map/all_to_all | solution.py:54
  46.1 2.5 %convert_element_type.39 = bf16[4,512,512]{2,1,0:T(8,128)(2,1)S(1)} convert(f32[4,512,512]{2,1,0:T(8,128)} %param.11) | non-fusion elementwise | flops 1048576 | bytes 6291456 | tf_op jit(solution)/shard_map/convert_element_type | solution.py:27
  48.7 1.6 pad_maximum_fusion
  50.3 3.8 %all-to-all-start = ((bf16[4,1,512,512]{3,2,1,0:T(8,128)(2,1)}), bf16[4,1,512,512]{3,2,1,0:T(8,128)(2,1)S(1)}, u32[]{:S(2)}, u32[]{:S(2)}) async-start(bf16[4,1,512,512]{3,2,1,0:T(8,128)(2,1)} %pad_maximum_fusion), calls=%async_computation | async-start | bytes 4194304 | tf_op jit(solution)/shard_map/all_to_all | solution.py:32
  54.1 6.8 %multiply_convert_fusion = (bf16[4,512,512]{2,1,0:T(8,128)(2,1)}, bf16[4,512,512]{2,1,0:T(8,128)(2,1)}) fusion(f32[4,512,512]{2,1,0:T(8,128)} %param.10, f32[512]{0:T(512)S(1)} %copy-done.1, f32[4,512,512]{2,1,0:T(8,128)} %param.9), kind=kLoop, calls=%fused_computation.1 | loop fusion | flops 4194304 | bytes 12584960 | tf_op jit(solution)/shard_map/convert_element_type | solution.py:26
  60.8 14.1 %all-to-all-done = bf16[4,1,512,512]{3,2,1,0:T(8,128)(2,1)S(1)} async-done(((bf16[4,1,512,512]{3,2,1,0:T(8,128)(2,1)}), bf16[4,1,512,512]{3,2,1,0:T(8,128)(2,1)S(1)}, u32[]{:S(2)}, u32[]{:S(2)}) %all-to-all-start) | async-done | bytes 2097184 | tf_op jit(solution)/shard_map/all_to_all | solution.py:32
  74.9 29.5 %all_to_all.40 = bf16[4,512,512]{2,1,0:T(8,128)(2,1)} all-to-all(bf16[4,512,512]{2,1,0:T(8,128)(2,1)} %get-tuple-element.9), channel_id=1, replica_groups=mesh['fs'=4,'tp'=8] {'fs'}, dimensions={0} | all-to-all | bytes 4194304 | tf_op jit(solution)/shard_map/all_to_all | solution.py:29
  104.4 4.5 %all-to-all-start.3 = ((bf16[4,512,512]{2,1,0:T(8,128)(2,1)}), bf16[4,512,512]{2,1,0:T(8,128)(2,1)}, u32[]{:S(2)}, u32[]{:S(2)}) async-start(bf16[4,512,512]{2,1,0:T(8,128)(2,1)} %get-tuple-element.8), calls=%async_computation.3 | async-start | bytes 4194304 | tf_op jit(solution)/shard_map/all_to_all | solution.py:30
  109.0 6.5 %fusion.5 = f32[1024,512]{1,0:T(8,128)} fusion(bf16[1024,2048]{1,0:T(8,128)(2,1)} %all-gather.2.cloned.1.call-done, bf16[2048,512]{1,0:T(8,128)(2,1)} %bitcast.39), kind=kOutput, calls=%fused_computation.34 | convolution fusion | flops 2147483648 | bytes 8388608 | tf_op jit(solution)/shard_map/dot_general | solution.py:60
  115.5 16.6 %all-to-all-done.3 = bf16[4,512,512]{2,1,0:T(8,128)(2,1)} async-done(((bf16[4,512,512]{2,1,0:T(8,128)(2,1)}), bf16[4,512,512]{2,1,0:T(8,128)(2,1)}, u32[]{:S(2)}, u32[]{:S(2)}) %all-to-all-start.3) | async-done | bytes 2097184 | tf_op jit(solution)/shard_map/all_to_all | solution.py:30
  132.0 10.1 %convolution_convert_fusion = bf16[2048,1024]{1,0:T(8,128)(2,1)} fusion(bf16[2048,512]{1,0:T(8,128)(2,1)S(1)} %bitcast.37, f32[1024,512]{1,0:T(8,128)} %fusion.5, bf16[1024,2048]{1,0:T(8,128)(2,1)} %all-gather.2.cloned.1.call-done, bf16[2048,512]{1,0:T(8,128)(2,1)} %bitcast.13), kind=kOutput, calls=%fused_computation.3 | convolution fusion | flops 4300210176 | bytes 14680064 | tf_op jit(solution)/shard_map/dot_general | solution.py:65
  142.2 53.7 %reduce-scatter.2.cloned.1.call-done = bf16[256,1024]{1,0:T(8,128)(2,1)} async-done(((bf16[2048,1024]{1,0:T(8,128)(2,1)}), bf16[256,1024]{1,0:T(8,128)(2,1)}) %reduce-scatter.2.cloned.1.call-update) | async-done | bytes 524304 | tf_op jit(solution)/shard_map/reduce_scatter | solution.py:64
  195.8 1.9 copy.40
  197.7 4.1 %all-to-all-start.4 = ((bf16[256,4,256]{2,0,1:T(8,128)(2,1)}), bf16[256,4,256]{2,0,1:T(8,128)(2,1)}, u32[]{:S(2)}, u32[]{:S(2)}) async-start(bf16[256,4,256]{2,0,1:T(8,128)(2,1)} %bitcast.36), calls=%async_computation.5 | async-start | bytes 1048576 | tf_op jit(solution)/shard_map/all_to_all | solution.py:74
  202.1 6.4 %all-to-all-done.4 = bf16[256,4,256]{2,0,1:T(8,128)(2,1)} async-done(((bf16[256,4,256]{2,0,1:T(8,128)(2,1)}), bf16[256,4,256]{2,0,1:T(8,128)(2,1)}, u32[]{:S(2)}, u32[]{:S(2)}) %all-to-all-start.4) | async-done | bytes 524320 | tf_op jit(solution)/shard_map/all_to_all | solution.py:74
  208.5 2.0 copy.37
  210.5 2.3 %convolution_convert_fusion.1 = bf16[256,256]{1,0:T(8,128)(2,1)} fusion(f32[256,1024]{1,0:T(8,128)S(1)} %select_reduce_fusion.1, bf16[256,1024]{0,1:T(8,128)(2,1)} %bitcast.42), kind=kOutput, calls=%fused_computation.9 | convolution fusion | flops 805371904 | bytes 1703936 | tf_op jit(solution)/shard_map/dot_general | solution.py:77
  212.8 3.0 %copy.44 = bf16[1,2048,512]{2,1,0:T(8,128)(2,1)} copy(bf16[1,2048,512]{2,1,0:T(8,128)(2,1)} %bitcast.40) | data formatting | bytes 4194304
  215.9 3.0 %copy.45 = bf16[1,2048,512]{2,1,0:T(8,128)(2,1)} copy(bf16[1,2048,512]{2,1,0:T(8,128)(2,1)} %bitcast.16) | data formatting | bytes 4194304
  218.9 1.3 copy.46
  (33 shorter events, 4.3 us)
Async XLA Ops:
  7.2 101.8 %all-gather.2.cloned.1.call-start = ((), (), s32[]{:S(2)}) async-start(), calls=%async_computation.6 | async-start | bytes 4718592 | tf_op jit(solution)/shard_map/all_gather | solution.py:59
  50.3 3.8 %copy-start.1 = (f32[512]{0:T(512)S(1)}, f32[512]{0:T(512)}, u32[]{:S(2)}) copy-start(f32[512]{0:T(512)} %param.8) | copy-start | bytes 6148
  50.3 24.6 %all-to-all-start = ((bf16[4,1,512,512]{3,2,1,0:T(8,128)(2,1)}), bf16[4,1,512,512]{3,2,1,0:T(8,128)(2,1)S(1)}, u32[]{:S(2)}, u32[]{:S(2)}) async-start(bf16[4,1,512,512]{3,2,1,0:T(8,128)(2,1)} %pad_maximum_fusion), calls=%async_computation | async-start | bytes 4194304 | tf_op jit(solution)/shard_map/all_to_all | solution.py:32
  104.4 27.6 %all-to-all-start.3 = ((bf16[4,512,512]{2,1,0:T(8,128)(2,1)}), bf16[4,512,512]{2,1,0:T(8,128)(2,1)}, u32[]{:S(2)}, u32[]{:S(2)}) async-start(bf16[4,512,512]{2,1,0:T(8,128)(2,1)} %get-tuple-element.8), calls=%async_computation.3 | async-start | bytes 4194304 | tf_op jit(solution)/shard_map/all_to_all | solution.py:30
  108.9 86.9 %reduce-scatter.2.cloned.1.call-start = ((), (), s32[]{:S(2)}) async-start(), calls=%async_computation.7 | async-start | bytes 4718592 | tf_op jit(solution)/shard_map/reduce_scatter | solution.py:64
  142.1 59.7 %copy-start = (f32[256,2]{0,1:T(2,128)S(1)}, f32[256,2]{0,1:T(2,128)}, u32[]{:S(2)}) copy-start(f32[256,2]{0,1:T(2,128)} %param.13) | copy-start | bytes 6148
  197.7 10.8 %all-to-all-start.4 = ((bf16[256,4,256]{2,0,1:T(8,128)(2,1)}), bf16[256,4,256]{2,0,1:T(8,128)(2,1)}, u32[]{:S(2)}, u32[]{:S(2)}) async-start(bf16[256,4,256]{2,0,1:T(8,128)(2,1)} %bitcast.36), calls=%async_computation.5 | async-start | bytes 1048576 | tf_op jit(solution)/shard_map/all_to_all | solution.py:74
Sparse Core Ops, SparseCore 0:
  46.2 44.4 all-gather.1
  142.3 53.5 reduce-scatter.1
